TPU v7x, 32 devices: a whole 2x2x4 slice. The times are simulated.
32 devices in a mesh: ep: 8 (over z, core), tp: 4 (over y, x).
Axes of the slice: x: 2, y: 2, z: 4, core: 2. Of those that a mesh axis runs over, the one named last changes fastest.
Arguments:
- tokens: bfloat16 [2048, 2048], P('ep'), may hold values from -6 to 6
- gate_proj: bfloat16 [8, 2048, 4096], P('ep', None, 'tp'), may hold values from -0.125 to 0.125
- up_proj: bfloat16 [8, 2048, 4096], P('ep', None, 'tp'), may hold values from -0.125 to 0.125
- down_proj: bfloat16 [8, 4096, 2048], P('ep', 'tp'), may hold values from -0.09375 to 0.09375
- side_input_weight: bfloat16 [2048, 1024], P(None, 'tp'), may hold values from -0.125 to 0.125
- dense_out: bfloat16 [1024, 2048], P(None, 'tp'), may hold values from -0.1875 to 0.1875
- dense_gate: bfloat16 [2048], replicated, may hold values from -0.125 to 0.125
- chosen_rows: int32 [8, 256], P(None, 'ep'), may hold values from 0 to 255, as said below
- choice_weights: float32 [8, 256], P(None, 'ep'), may hold values from 0.25 to 1
Outputs:
- mixed: bfloat16 [2048, 2048], P('ep', 'tp')
Inputs may be any that keep to these rules, and one draw needn't show every extreme that they name: `chosen_rows`: for each expert and each block of 32 columns (one index of ep), the 32 rows are distinct rows of that index's 256 tokens; every expert reads exactly 32 tokens of every index.
All inputs are finite; a program needn't handle non-finite values.
Results may differ from a plain program's by a relative error of at most 0.015.
Values may be sent and summed in bfloat16 or wider, within the bound.
A program may use at most 64 MiB of HBM per device.

v0:
```python
import jax
import jax.numpy as jnp
from jax import lax
from jax.sharding import PartitionSpec as P


def per_device(
    tokens,
    gate_proj,
    up_proj,
    down_proj,
    side_input_weight,
    dense_out,
    dense_gate,
    chosen_rows,
    choice_weights,
):
    tok_rows = tokens.shape[0]
    width = tokens.shape[1] // lax.axis_size("tp")
    column_position = lax.axis_index("tp") * width
    own_cols = lax.dynamic_slice_in_dim(tokens, column_position, width, 1)
    expert_count, slot_rows = chosen_rows.shape
    capacity = expert_count * slot_rows
    picked = jnp.take(own_cols, chosen_rows.reshape(-1), axis=0).reshape(
        expert_count, slot_rows, width
    )
    arrived = lax.all_to_all(picked, "ep", split_axis=0, concat_axis=1, tiled=True).reshape(
        capacity, width
    )
    w_gate = gate_proj[0]
    w_up = up_proj[0]
    w_down = down_proj[0]
    piece = lax.all_gather(arrived, "tp", axis=1, tiled=True)
    gate_val = jnp.dot(piece, w_gate, preferred_element_type=jnp.float32)
    up_val = jnp.dot(piece, w_up, preferred_element_type=jnp.float32)
    hidden = (jax.nn.silu(gate_val) * up_val).astype(jnp.bfloat16)
    summed = lax.psum_scatter(
        lax.dot_general(
            w_down, hidden, (((0,), (1,)), ((), ())), preferred_element_type=jnp.float32
        ).astype(jnp.bfloat16),
        "tp",
        scatter_dimension=0,
        tiled=True,
    )
    returned = lax.all_to_all(summed, "ep", split_axis=1, concat_axis=1, tiled=True)
    hits = (
        chosen_rows.reshape(-1)[:, None] == jnp.arange(tok_rows, dtype=jnp.int32)[None, :]
    ).astype(jnp.bfloat16)
    scaled = returned.astype(jnp.float32) * choice_weights.reshape(-1)[None, :]
    high_part = scaled.astype(jnp.bfloat16)
    lower_half = (scaled - high_part.astype(jnp.float32)).astype(jnp.bfloat16)
    contract = (((0,), (1,)), ((), ()))
    routed = lax.dot_general(
        hits, high_part, contract, preferred_element_type=jnp.float32
    ) + lax.dot_general(hits, lower_half, contract, preferred_element_type=jnp.float32)
    dense_hidden = jax.nn.silu(
        jnp.dot(tokens, side_input_weight, preferred_element_type=jnp.float32)
    ).astype(jnp.bfloat16)
    dense_val = jnp.dot(
        lax.all_gather(dense_hidden, "tp", axis=1, tiled=True),
        dense_out,
        preferred_element_type=jnp.float32,
    )
    side_gate = jax.nn.sigmoid(jnp.dot(tokens, dense_gate, preferred_element_type=jnp.float32))
    return (routed + side_gate[:, None] * dense_val).astype(jnp.bfloat16)


def solution(mesh):
    placed = (
        P("ep", None),
        P("ep", None, "tp"),
        P("ep", None, "tp"),
        P("ep", "tp", None),
        P(None, "tp"),
        P(None, "tp"),
        P(),
        P(None, "ep"),
        P(None, "ep"),
    )
    return jax.shard_map(
        per_device, mesh=mesh, in_specs=placed, out_specs=P("ep", "tp"), check_vma=False
    )
```

profile of v0, /device:TPU:0, one launch (start us, length us, event | category | flops | bytes accessed | tf_op | source)
XLA Modules:
  0.0 116.5 jit_solution(18036005292770435474)
XLA Ops:
  6.5 0.0 copy-start
  6.5 0.0 all-gather.2.cloned.1.call-start
  6.5 0.9 reshape.57
  7.4 0.7 compare_and_fusion
  8.1 0.0 copy-done
  8.1 1.2 gather_fusion
  9.3 0.1 broadcast_select_fusion
  9.4 16.0 %all_to_all.18 = bf16[8,32,512]{2,1,0:T(8,128)(2,1)} all-to-all(bf16[8,32,512]{2,1,0:T(8,128)(2,1)S(1)} %broadcast_select_fusion), channel_id=1, replica_groups=mesh['ep'=8,'tp'=4] {'ep'}, dimensions={0} | all-to-all | bytes 524288 | tf_op jit(solution)/shard_map/all_to_all | solution.py:27
  25.4 0.0 all-gather.2.cloned.1.call-update
  25.4 0.0 reduce-scatter.2.cloned.1.call-start
  25.4 25.4 %all-gather.2.cloned.1.call-done = bf16[256,2048]{1,0:T(8,128)(2,1)} async-done(((bf16[256,512]{1,0:T(8,128)(2,1)}), bf16[256,2048]{1,0:T(8,128)(2,1)}) %all-gather.2.cloned.1.call-update) | async-done | bytes 1048592 | tf_op jit(solution)/shard_map/all_gather | solution.py:33
  50.9 3.8 %fusion.4 = f32[256,1024]{1,0:T(8,128)S(1)} fusion(bf16[256,2048]{1,0:T(8,128)(2,1)} %all-gather.2.cloned.1.call-done, bf16[1,2048,1024]{2,1,0:T(8,128)(2,1)} %param.10), kind=kOutput, calls=%fused_computation.5 | convolution fusion | flops 1073741824 | bytes 6291456 | tf_op jit(solution)/shard_map/dot_general | solution.py:34
  54.7 0.0 copy-done.5
  54.7 0.0 copy-start.2
  54.7 0.0 copy-start.4
  54.7 0.0 copy-start.3
  54.7 6.9 %fusion.9 = bf16[2048,256]{0,1:T(8,128)(2,1)} fusion(bf16[1,1024,2048]{2,1,0:T(8,128)(2,1)} %param.12, bf16[256,2048]{1,0:T(8,128)(2,1)S(1)} %copy-done.5, bf16[1,2048,1024]{2,1,0:T(8,128)(2,1)} %param.11, f32[256,1024]{1,0:T(8,128)S(1)} %fusion.4), kind=kOutput, calls=%fused_computation.8 | convolution fusion | flops 2149580800 | bytes 11534336 | tf_op jit(solution)/shard_map/dot_general | solution.py:38
  61.7 0.0 reduce-scatter.2.cloned.1.call-update
  61.7 0.0 copy-done.2
  61.7 0.1 eq.15
  61.8 0.1 mul.35
  61.9 0.0 copy-start.1
  61.9 1.8 %multiply_convert_fusion = bf16[256,256]{1,0:T(8,128)(2,1)S(1)} fusion(bf16[256,2048]{1,0:T(8,128)(2,1)S(1)} %copy-done, bf16[2048,256]{1,0:T(8,128)(2,1)} %param.13), kind=kOutput, calls=%fused_computation.20 | convolution fusion | flops 268763136 | bytes 2228224 | tf_op jit(solution)/shard_map/dot_general | solution.py:57
  63.6 17.9 %all_gather.7 = bf16[256,1024]{1,0:T(8,128)(2,1)S(1)} all-gather(bf16[256,256]{1,0:T(8,128)(2,1)S(1)} %multiply_convert_fusion), channel_id=1, replica_groups=mesh['ep'=8,'tp'=4] {'tp'}, dimensions={1}, use_global_device_ids=true | all-gather | bytes 655360 | tf_op jit(solution)/shard_map/all_gather | solution.py:60
  81.6 11.8 %reduce-scatter.2.cloned.1.call-done = bf16[512,256]{0,1:T(8,128)(2,1)} async-done(((bf16[2048,256]{0,1:T(8,128)(2,1)}), bf16[512,256]{0,1:T(8,128)(2,1)}) %reduce-scatter.2.cloned.1.call-update) | async-done | bytes 262160 | tf_op jit(solution)/shard_map/reduce_scatter | solution.py:37
  93.3 4.6 %all-to-all-start.1 = ((bf16[512,8,32]{0,2,1:T(8,128)(2,1)}), bf16[512,8,32]{0,2,1:T(8,128)(2,1)S(1)}, u32[]{:S(2)}, u32[]{:S(2)}) async-start(bf16[512,8,32]{0,2,1:T(8,128)(2,1)} %bitcast.41), calls=%async_computation.2 | async-start | bytes 524288 | tf_op jit(solution)/shard_map/all_to_all | solution.py:45
  97.9 0.4 fusion.32
  98.3 9.3 %all-to-all-done.1 = bf16[512,8,32]{0,2,1:T(8,128)(2,1)S(1)} async-done(((bf16[512,8,32]{0,2,1:T(8,128)(2,1)}), bf16[512,8,32]{0,2,1:T(8,128)(2,1)S(1)}, u32[]{:S(2)}, u32[]{:S(2)}) %all-to-all-start.1) | async-done | bytes 262176 | tf_op jit(solution)/shard_map/all_to_all | solution.py:45
  107.7 0.1 fusion.23
  107.8 0.3 fusion.28
  108.1 0.4 convolution_add_fusion
  108.5 1.1 fusion.19
  (9 shorter events, 0.1 us)
Async XLA Ops:
  6.5 1.6 %copy-start = (bf16[256,2048]{1,0:T(8,128)(2,1)S(1)}, bf16[256,2048]{1,0:T(8,128)(2,1)}, u32[]{:S(2)}) copy-start(bf16[256,2048]{1,0:T(8,128)(2,1)} %param.9) | copy-start | bytes 3145732
  6.5 44.3 %all-gather.2.cloned.1.call-start = ((), (), s32[]{:S(2)}) async-start(), calls=%async_computation.3 | async-start | bytes 1310720 | tf_op jit(solution)/shard_map/all_gather | solution.py:33
  25.4 67.9 %reduce-scatter.2.cloned.1.call-start = ((), (), s32[]{:S(2)}) async-start(), calls=%async_computation.4 | async-start | bytes 1310720 | tf_op jit(solution)/shard_map/reduce_scatter | solution.py:37
  50.9 3.8 %copy-start.5 = (bf16[256,2048]{1,0:T(8,128)(2,1)S(1)}, bf16[256,2048]{1,0:T(8,128)(2,1)}, u32[]{:S(2)}) copy-start(bf16[256,2048]{1,0:T(8,128)(2,1)} %all-gather.2.cloned.1.call-done) | copy-start | bytes 3145732
  54.7 7.0 %copy-start.2 = (s32[8,32]{1,0:T(8,128)S(1)}, s32[8,32]{1,0:T(8,128)}, u32[]{:S(2)}) copy-start(s32[8,32]{1,0:T(8,128)} %param.16) | copy-start | bytes 3076
  54.7 7.0 %copy-start.4 = (f32[8,32]{1,0:T(8,128)S(1)}, f32[8,32]{1,0:T(8,128)}, u32[]{:S(2)}) copy-start(f32[8,32]{1,0:T(8,128)} %param.17) | copy-start | bytes 3076
  54.7 7.1 %copy-start.3 = (bf16[2048]{0:T(1024)(128)(2,1)S(1)}, bf16[2048]{0:T(1024)(128)(2,1)}, u32[]{:S(2)}) copy-start(bf16[2048]{0:T(1024)(128)(2,1)} %param.15) | copy-start | bytes 12292
  61.9 46.7 %copy-start.1 = (bf16[1024,512]{1,0:T(8,128)(2,1)S(1)}, bf16[1024,512]{1,0:T(8,128)(2,1)}, u32[]{:S(2)}) copy-start(bf16[1024,512]{1,0:T(8,128)(2,1)} %param.14) | copy-start | bytes 3145732
  93.3 14.3 %all-to-all-start.1 = ((bf16[512,8,32]{0,2,1:T(8,128)(2,1)}), bf16[512,8,32]{0,2,1:T(8,128)(2,1)S(1)}, u32[]{:S(2)}, u32[]{:S(2)}) async-start(bf16[512,8,32]{0,2,1:T(8,128)(2,1)} %bitcast.41), calls=%async_computation.2 | async-start | bytes 524288 | tf_op jit(solution)/shard_map/all_to_all | solution.py:45
Sparse Core Ops, SparseCore 0:
  25.5 25.2 all-gather.1
  61.8 31.4 reduce-scatter.1
where the time goes:
time: 117 us
  waiting for transfers between devices  46.5 us (40%)
  blocking collectives  33.9 us (29%)
  matrix products  14.8 us (13%)
  between operations  13.5 us (12%)
  starting transfers between devices  4.65 us (4%)
  local copies, waits for them, and re-layouts  2.23 us (2%)
    all_gather x1, waiting for transfers between devices, per_device(): piece = lax.all_gather(arrived, 'tp', axis=1, tiled=True)  25.4 us
    all_gather x1, blocking collectives, per_device(): lax.all_gather(dense_hidden, 'tp', axis=1, tiled=True)  17.9 us
    all_to_all x1, blocking collectives, per_device(): lax.all_to_all(picked, 'ep', split_axis=0, concat_axis=1, tiled=True)  16 us
    reduce_scatter x1, waiting for transfers between devices, per_device(): lax.psum_scatter(lax.dot_general(w_down, hidden, (((0,), (1,)), ((), ()))...  11.8 us
    all_to_all x1, waiting for transfers between devices, per_device(): lax.all_to_all(summed, 'ep', split_axis=1, concat_axis=1, tiled=True)  9.33 us
    dot_general x1, matrix products, per_device(): lax.dot_general(w_down, hidden, (((0,), (1,)), ((), ())), preferred_eleme...  6.9 us
    all_to_all x1, starting transfers between devices, per_device(): lax.all_to_all(summed, 'ep', split_axis=1, concat_axis=1, tiled=True)  4.61 us
    dot_general x1, matrix products, per_device(): gate_val = jnp.dot(piece, w_gate, preferred_element_type=jnp.float32)  3.83 us
  transfers between devices with their start and end apart: 3, of which 3 were waited for; matrix products, arithmetic and copies ran while one was open for 2% of the time, Pallas kernels for 0%

commit v1 on v0

--- a/solution.py
+++ b/solution.py
@@ -1,10 +1,17 @@
+import functools
+
 import jax
 import jax.numpy as jnp
 from jax import lax
+from jax.experimental import pallas as pl
+from jax.experimental.pallas import tpu as pltpu
 from jax.sharding import PartitionSpec as P
 
-
-def per_device(
+MESH = pl.DeviceIdType.MESH
+LANES = 128
+
+
+def plain_per_device(
     tokens,
     gate_proj,
     up_proj,
@@ -27,16 +34,13 @@
     arrived = lax.all_to_all(picked, "ep", split_axis=0, concat_axis=1, tiled=True).reshape(
         capacity, width
     )
-    w_gate = gate_proj[0]
-    w_up = up_proj[0]
-    w_down = down_proj[0]
     piece = lax.all_gather(arrived, "tp", axis=1, tiled=True)
-    gate_val = jnp.dot(piece, w_gate, preferred_element_type=jnp.float32)
-    up_val = jnp.dot(piece, w_up, preferred_element_type=jnp.float32)
+    gate_val = jnp.dot(piece, gate_proj[0], preferred_element_type=jnp.float32)
+    up_val = jnp.dot(piece, up_proj[0], preferred_element_type=jnp.float32)
     hidden = (jax.nn.silu(gate_val) * up_val).astype(jnp.bfloat16)
     summed = lax.psum_scatter(
         lax.dot_general(
-            w_down, hidden, (((0,), (1,)), ((), ())), preferred_element_type=jnp.float32
+            down_proj[0], hidden, (((0,), (1,)), ((), ())), preferred_element_type=jnp.float32
         ).astype(jnp.bfloat16),
         "tp",
         scatter_dimension=0,
@@ -65,6 +69,415 @@
     return (routed + side_gate[:, None] * dense_val).astype(jnp.bfloat16)
 
 
+def dot(a, b):
+    return jnp.dot(a, b, preferred_element_type=jnp.float32)
+
+
+def silu(v):
+    return v / (1.0 + jnp.exp(-v))
+
+
+def layer_kernel(
+    n_ep,
+    slot,
+    tok_hbm,
+    gate_hbm,
+    up_hbm,
+    down_hbm,
+    side_hbm,
+    dout_hbm,
+    dgate_ref,
+    rows_ref,
+    cw_ref,
+    out_ref,
+    tok,
+    w_gate,
+    w_up,
+    w_down,
+    w_side,
+    w_dout,
+    pick,
+    xin,
+    g_acc,
+    u_acc,
+    hid,
+    comb,
+    dhid,
+    part,
+    d_in,
+    rx,
+    ry,
+    pair,
+    fin,
+    back,
+    load_sem,
+    send_sem,
+    z_sem,
+    ag_sem,
+    dh_sem,
+    rsd_sem,
+    rsx_sem,
+    rsy_sem,
+    ret_sem,
+):
+    e = lax.axis_index("ep")
+    p = lax.axis_index("tp")
+    px = p + 1 - 2 * (p % 2)
+    py = p + 2 - 4 * (p // 2)
+    pd = px + 2 - 4 * (px // 2)
+    z = e // 2
+    nz = n_ep // 2
+    width = xin.shape[2]
+    tok_rows = tok.shape[0]
+    side = w_side.shape[1]
+    to_x, to_y = {"tp": px}, {"tp": py}
+
+    loads = []
+    for i, (src, dst) in enumerate(
+        (
+            (tok_hbm, tok),
+            (side_hbm, w_side),
+            (gate_hbm.at[0], w_gate),
+            (up_hbm.at[0], w_up),
+            (down_hbm.at[0], w_down),
+            (dout_hbm, w_dout),
+        )
+    ):
+        copy = pltpu.make_async_copy(src, dst, load_sem.at[i])
+        copy.start()
+        loads.append(copy)
+
+    barrier = pltpu.get_barrier_semaphore()
+    for k in range(1, n_ep):
+        pl.semaphore_signal(
+            barrier, inc=1, device_id={"ep": (e + k) % n_ep}, device_id_type=MESH
+        )
+    for there in (to_x, to_y):
+        pl.semaphore_signal(barrier, inc=1, device_id=there, device_id_type=MESH)
+
+    def block(owner):
+        return pl.ds(pl.multiple_of(owner * slot, slot), slot)
+
+    sends = []
+
+    def send(src, dst, sem, there):
+        copy = pltpu.make_async_remote_copy(
+            src_ref=src,
+            dst_ref=dst,
+            send_sem=send_sem.at[len(sends)],
+            recv_sem=sem,
+            device_id=there,
+            device_id_type=MESH,
+        )
+        copy.start()
+        sends.append(copy)
+
+    def arrive(dst, sem):
+        pltpu.make_async_remote_copy(
+            src_ref=dst,
+            dst_ref=dst,
+            send_sem=send_sem.at[0],
+            recv_sem=sem,
+            device_id=to_x,
+            device_id_type=MESH,
+        ).wait_recv()
+
+    rows_t = rows_ref[...].astype(jnp.float32).T
+    cw_t = cw_ref[...].T
+    lane = lax.broadcasted_iota(jnp.int32, (slot, tok_rows), 1).astype(jnp.float32)
+    hits = jnp.concatenate(
+        [jnp.where(rows_t[:, k : k + 1] == lane, 1.0, 0.0) for k in range(n_ep)], axis=0
+    )
+    loads[0].wait()
+    own = pl.ds(pl.multiple_of(p * width, width), width)
+    pick[...] = dot(hits.astype(jnp.bfloat16), tok[:, own]).astype(jnp.bfloat16)
+    pl.semaphore_wait(barrier, n_ep + 1)
+
+    far = sorted(range(1, n_ep), key=lambda k: -min(k, n_ep - k))
+    for k in far:
+        peer = (e + k) % n_ep
+        send(pick.at[block(peer)], xin.at[p, block(e)], z_sem.at[e], {"ep": peer})
+    xin[p, block(e)] = pick[block(e), :]
+
+    def spread(owner):
+        ref = xin.at[p, block(owner)]
+        send(ref, ref, ag_sem.at[0, owner], to_x)
+        send(ref, ref, ag_sem.at[1, owner], to_y)
+
+    spread(e)
+
+    loads[1].wait()
+    dhid[p] = silu(dot(tok[...], w_side[...])).astype(jnp.bfloat16)
+    send(dhid.at[p], dhid.at[p], dh_sem.at[0], to_x)
+    send(dhid.at[p], dhid.at[p], dh_sem.at[1], to_y)
+
+    weight = jnp.concatenate([cw_t[:, k : k + 1] for k in range(n_ep)], axis=0)
+    both = (hits * weight).T
+    high = both.astype(jnp.bfloat16)
+    comb[0] = high
+    comb[1] = (both - high.astype(jnp.float32)).astype(jnp.bfloat16)
+
+    near = [n_ep - k for k in far[::-1]]
+    near = sorted(range(1, n_ep), key=lambda k: min(k, n_ep - k))
+    for k in near:
+        owner = (e + n_ep - k) % n_ep
+        arrive(xin.at[p, block(owner)], z_sem.at[owner])
+        spread(owner)
+
+    tile = 2 * LANES
+    n_tiles = g_acc.shape[1] // tile
+
+    loads[2].wait()
+    loads[3].wait()
+
+    def gate_up(q, first):
+        rows = pl.ds(pl.multiple_of(q * width, width), width)
+
+        @pl.loop(0, n_tiles)
+        def _(n):
+            cols = pl.ds(pl.multiple_of(n * tile, tile), tile)
+            g = dot(xin[q], w_gate[rows, cols])
+            u = dot(xin[q], w_up[rows, cols])
+            if first:
+                g_acc[:, cols] = g
+                u_acc[:, cols] = u
+            else:
+                g_acc[:, cols] += g
+                u_acc[:, cols] += u
+
+    gate_up(p, True)
+
+    order = [0] + near
+    zs = [j for j in range(nz)]
+    for j in zs:
+        zo = (z + j) % nz
+        even, odd = 2 * zo, 2 * zo + 1
+        ref = xin.at[px, block(even)]
+        arrive(ref, ag_sem.at[0, even])
+        send(ref, ref, ag_sem.at[2, even], to_y)
+        ref = xin.at[py, block(odd)]
+        arrive(ref, ag_sem.at[1, odd])
+        send(ref, ref, ag_sem.at[2, odd], to_x)
+    half = tok_rows // 2
+    arrive(dhid.at[px], dh_sem.at[0])
+    ref = dhid.at[px, pl.ds(0, half)]
+    send(ref, ref, dh_sem.at[2], to_y)
+    arrive(dhid.at[py], dh_sem.at[1])
+    ref = dhid.at[py, pl.ds(half, half)]
+    send(ref, ref, dh_sem.at[3], to_x)
+
+    for j in zs:
+        odd = 2 * j + 1
+        arrive(xin.at[px, block(odd)], ag_sem.at[0, odd])
+    gate_up(px, False)
+    for j in zs:
+        even = 2 * j
+        arrive(xin.at[py, block(even)], ag_sem.at[1, even])
+    gate_up(py, False)
+    for owner in range(n_ep):
+        arrive(xin.at[pd, block(owner)], ag_sem.at[2, owner])
+
+    last = pl.ds(pl.multiple_of(pd * width, width), width)
+
+    @pl.loop(0, n_tiles)
+    def _(n):
+        cols = pl.ds(pl.multiple_of(n * tile, tile), tile)
+        g = g_acc[:, cols] + dot(xin[pd], w_gate[last, cols])
+        u = u_acc[:, cols] + dot(xin[pd], w_up[last, cols])
+        hid[:, cols] = (silu(g) * u).astype(jnp.bfloat16)
+
+    loads[4].wait()
+
+    def down(at, q):
+        @pl.loop(0, width // tile)
+        def _(n):
+            cols = pl.ds(pl.multiple_of(n * tile, tile), tile)
+            src = pl.ds(pl.multiple_of(q * width + n * tile, tile), tile)
+            part[at, :, cols] = dot(hid[...], w_down[:, src]).astype(jnp.bfloat16)
+
+    offs = sorted(range(nz), key=lambda j: (-min(j, nz - j), j))
+
+    def pieces(g):
+        zo = (z + offs[g]) % nz
+        return 2 * zo, 2 * zo + 1
+
+    def first_d(g):
+        even, odd = pieces(g)
+        send(part.at[3, block(odd)], d_in.at[block(odd)], rsd_sem.at[odd], to_x)
+        send(part.at[3, block(even)], d_in.at[block(even)], rsd_sem.at[even], to_y)
+
+    def direct_x(g):
+        odd = pieces(g)[1]
+        send(part.at[1, block(odd)], rx.at[block(odd)], rsx_sem.at[odd], to_x)
+
+    def direct_y(g):
+        even = pieces(g)[0]
+        send(part.at[2, block(even)], ry.at[block(even)], rsy_sem.at[even], to_y)
+
+    def direct(g):
+        first_d(g)
+        direct_x(g)
+        direct_y(g)
+
+    f32 = jnp.float32
+
+    def joined(g):
+        even, odd = pieces(g)
+        for owner, at, dst, sem, there in (
+            (even, 1, rx, rsx_sem, to_x),
+            (odd, 2, ry, rsy_sem, to_y),
+        ):
+            b = block(owner)
+            arrive(d_in.at[b], rsd_sem.at[owner])
+            pair[b, :] = (part[at, b, :].astype(f32) + d_in[b, :].astype(f32)).astype(
+                jnp.bfloat16
+            )
+            send(pair.at[b], dst.at[b], sem.at[owner], there)
+
+    def finish(g):
+        even, odd = pieces(g)
+        for owner in (even, odd):
+            b = block(owner)
+            arrive(rx.at[b], rsx_sem.at[owner])
+            arrive(ry.at[b], rsy_sem.at[owner])
+            fin[b, :] = (
+                part[0, b, :].astype(f32) + rx[b, :].astype(f32) + ry[b, :].astype(f32)
+            ).astype(jnp.bfloat16)
+            if offs[g]:
+                send(fin.at[b], back.at[block(e)], ret_sem.at[e], {"ep": owner})
+        if not offs[g]:
+            other = e + 1 - 2 * (e % 2)
+            send(fin.at[block(other)], back.at[block(e)], ret_sem.at[e], {"ep": other})
+            back[block(e), :] = fin[block(e), :]
+
+    down(3, pd)
+    first_d(0)
+    down(1, px)
+    direct_x(0)
+    down(2, py)
+    direct_y(0)
+    if nz > 1:
+        direct(1)
+    down(0, p)
+
+    for g in range(nz):
+        joined(g)
+        if g + 2 < nz:
+            direct(g + 2)
+        if g >= 1:
+            finish(g - 1)
+        if g == min(1, nz - 1):
+            arrive(dhid.at[pd, pl.ds(0, half)], dh_sem.at[2])
+            arrive(dhid.at[pd, pl.ds(half, half)], dh_sem.at[3])
+            loads[5].wait()
+            total = dot(dhid[0], w_dout[pl.ds(0, side)])
+            for q in range(1, dhid.shape[0]):
+                total += dot(dhid[q], w_dout[pl.ds(q * side, side)])
+            logit = jnp.sum(
+                tok[...].astype(f32) * dgate_ref[...].astype(f32), axis=1, keepdims=True
+            )
+            g_acc[:, pl.ds(0, width)] = total / (1.0 + jnp.exp(-logit))
+    finish(nz - 1)
+
+    for k in near:
+        owner = (e + n_ep - k) % n_ep
+        arrive(back.at[block(owner)], ret_sem.at[owner])
+    out_ref[...] = (
+        g_acc[:, pl.ds(0, width)] + dot(comb[0], back[...]) + dot(comb[1], back[...])
+    ).astype(jnp.bfloat16)
+    for copy in sends:
+        copy.wait_send()
+
+
+def fused_per_device(
+    tokens,
+    gate_proj,
+    up_proj,
+    down_proj,
+    side_input_weight,
+    dense_out,
+    dense_gate,
+    chosen_rows,
+    choice_weights,
+):
+    n_ep, slot = chosen_rows.shape
+    n_tp = lax.axis_size("tp")
+    tok_rows, d = tokens.shape
+    width = d // n_tp
+    ff = gate_proj.shape[2]
+    side = side_input_weight.shape[1]
+    cap = n_ep * slot
+    bf16, f32 = jnp.bfloat16, jnp.float32
+    n_sends = 2 * (n_ep - 1) + 2 * n_ep + n_ep + 4 + 3 * n_ep
+    hbm = pl.BlockSpec(memory_space=pltpu.HBM)
+    vmem = pl.BlockSpec(memory_space=pltpu.VMEM)
+    return pl.pallas_call(
+        functools.partial(layer_kernel, n_ep, slot),
+        out_shape=jax.ShapeDtypeStruct((tok_rows, width), bf16),
+        in_specs=[hbm] * 6 + [vmem] * 3,
+        out_specs=vmem,
+        scratch_shapes=[
+            pltpu.VMEM((tok_rows, d), bf16),
+            pltpu.VMEM((d, ff), bf16),
+            pltpu.VMEM((d, ff), bf16),
+            pltpu.VMEM((ff, d), bf16),
+            pltpu.VMEM((d, side), bf16),
+            pltpu.VMEM((n_tp * side, width), bf16),
+            pltpu.VMEM((cap, width), bf16),
+            pltpu.VMEM((n_tp, cap, width), bf16),
+            pltpu.VMEM((cap, ff), f32),
+            pltpu.VMEM((cap, ff), f32),
+            pltpu.VMEM((cap, ff), bf16),
+            pltpu.VMEM((2, tok_rows, cap), bf16),
+            pltpu.VMEM((n_tp, tok_rows, side), bf16),
+            pltpu.VMEM((4, cap, width), bf16),
+            pltpu.VMEM((cap, width), bf16),
+            pltpu.VMEM((cap, width), bf16),
+            pltpu.VMEM((cap, width), bf16),
+            pltpu.VMEM((cap, width), bf16),
+            pltpu.VMEM((cap, width), bf16),
+            pltpu.VMEM((cap, width), bf16),
+            pltpu.SemaphoreType.DMA((6,)),
+            pltpu.SemaphoreType.DMA((n_sends,)),
+            pltpu.SemaphoreType.DMA((n_ep,)),
+            pltpu.SemaphoreType.DMA((3, n_ep)),
+            pltpu.SemaphoreType.DMA((4,)),
+            pltpu.SemaphoreType.DMA((n_ep,)),
+            pltpu.SemaphoreType.DMA((n_ep,)),
+            pltpu.SemaphoreType.DMA((n_ep,)),
+            pltpu.SemaphoreType.DMA((n_ep,)),
+        ],
+        compiler_params=pltpu.CompilerParams(collective_id=0, has_side_effects=True),
+    )(
+        tokens,
+        gate_proj,
+        up_proj,
+        down_proj,
+        side_input_weight,
+        dense_out,
+        dense_gate.reshape(1, d),
+        chosen_rows,
+        choice_weights,
+    )
+
+
+def per_device(*args):
+    tokens, gate_proj, chosen_rows = args[0], args[1], args[7]
+    n_ep, slot = chosen_rows.shape
+    n_tp = lax.axis_size("tp")
+    width, tile = tokens.shape[1] // n_tp, 2 * LANES
+    fits = (
+        n_tp == 4
+        and n_ep % 2 == 0
+        and tokens.shape[0] == n_ep * slot
+        and slot % 16 == 0
+        and width % tile == 0
+        and gate_proj.shape[2] % tile == 0
+        and args[4].shape[1] % LANES == 0
+    )
+    return fused_per_device(*args) if fits else plain_per_device(*args)
+
+
 def solution(mesh):
     placed = (
         P("ep", None),

time: 117 us -> 43.9 us (0.38)
  waiting for transfers between devices: 46.5 us -> 0 us
  Pallas kernels: 0 us -> 40.6 us
  blocking collectives: 33.9 us -> 0 us
  matrix products: 14.8 us -> 0 us
  between operations: 13.5 us -> 0.01 us
  starting transfers between devices: 4.65 us -> 0 us
    pallas_call x0 -> x1, Pallas kernels: none -> 40.6 us  [fused_per_device(): pl.pallas_call(functools.partial(layer_kernel, n_ep, slot), out_shape=jax...]
    all_gather x1 -> x0, waiting for transfers between devices: 25.4 us -> none  [per_device(): piece = lax.all_gather(arrived, 'tp', axis=1, tiled=True)]
    all_gather x1 -> x0, blocking collectives: 17.9 us -> none  [per_device(): lax.all_gather(dense_hidden, 'tp', axis=1, tiled=True)]
    all_to_all x1 -> x0, blocking collectives: 16 us -> none  [per_device(): lax.all_to_all(picked, 'ep', split_axis=0, concat_axis=1, tiled=True)]
    dot_general x7 -> x0, matrix products: 14.8 us -> none  [the longest x1 6.9 us: per_device(): lax.dot_general(w_down, hidden, (((0,), (1,)), ((), ())), preferred_eleme...]
    reduce_scatter x1 -> x0, waiting for transfers between devices: 11.8 us -> none  [per_device(): lax.psum_scatter(lax.dot_general(w_down, hidden, (((0,), (1,)), ((), ()))...]
    all_to_all x1 -> x0, waiting for transfers between devices: 9.33 us -> none  [per_device(): lax.all_to_all(summed, 'ep', split_axis=1, concat_axis=1, tiled=True)]
    all_to_all x1 -> x0, starting transfers between devices: 4.61 us -> none  [per_device(): lax.all_to_all(summed, 'ep', split_axis=1, concat_axis=1, tiled=True)]
  transfers between devices with their start and end apart: 3 -> 0, of which waited for: 3 -> 0; matrix products, arithmetic and copies ran while one was open for 2% -> 0% of each run, Pallas kernels for 0% -> 0%
where the time goes in v1:
time: 43.9 us; the launch traced here: 43.6 us
  Pallas kernels  40.6 us (92%)
  local copies, waits for them, and re-layouts  2.96 us (7%)
    pallas_call x1, Pallas kernels, fused_per_device(): pl.pallas_call(functools.partial(layer_kernel, n_ep, slot), out_shape=jax...  40.6 us
    unnamed x1, local copies, waits for them, and re-layouts  1.67 us
    reshape x1, local copies, waits for them, and re-layouts, fused_per_device(): dense_gate.reshape(1, d)  1.29 us

profile of v1, /device:TPU:0, one launch (start us, length us, event | category | flops | bytes accessed | tf_op | source)
XLA Modules:
  0.0 43.6 jit_solution(8829703575539980919)
XLA Ops:
  0.0 1.3 %reshape.3.dgate_ref = bf16[1,2048]{1,0:T(2,128)(2,1)} reshape(bf16[2048]{0:T(1024)(128)(2,1)} %param.15) | data formatting | bytes 8192 | tf_op jit(solution)/shard_map/reshape | solution.py:458
  1.3 40.6 %shard_map.91 = bf16[256,512]{1,0:T(8,128)(2,1)} custom-call(bf16[256,2048]{1,0:T(8,128)(2,1)} %tok_hbm.1, bf16[1,2048,1024]{2,1,0:T(8,128)(2,1)} %gate_hbm.1, bf16[1,2048,1024]{2,1,0:T(8,128)(2,1)} %up_hbm.1, bf16[1,1024,2048]{2,1,0:T(8,128)(2,1)} %down_hbm.1, bf16[2048,256]{1,0:T(8,128)(2,1)} %side_hbm.1, bf16[1024,512]{1,0:T(8,128)(2,1)} %dout_hbm.1, ...), custom_call_target="tpu_custom_call" | custom-call | tf_op jit(solution)/shard_map/pallas_call | solution.py:414
  41.9 1.7 %copy.11 = bf16[256,512]{1,0:T(8,128)(2,1)} copy(bf16[256,512]{1,0:T(8,128)(2,1)} %shard_map.91) | data formatting | bytes 524288

commit v2 on v1

--- a/solution.py
+++ b/solution.py
@@ -193,21 +193,52 @@
     pick[...] = dot(hits.astype(jnp.bfloat16), tok[:, own]).astype(jnp.bfloat16)
     pl.semaphore_wait(barrier, n_ep + 1)
 
-    far = sorted(range(1, n_ep), key=lambda k: -min(k, n_ep - k))
-    for k in far:
-        peer = (e + k) % n_ep
-        send(pick.at[block(peer)], xin.at[p, block(e)], z_sem.at[e], {"ep": peer})
-    xin[p, block(e)] = pick[block(e), :]
-
-    def spread(owner):
-        ref = xin.at[p, block(owner)]
-        send(ref, ref, ag_sem.at[0, owner], to_x)
-        send(ref, ref, ag_sem.at[1, owner], to_y)
-
-    spread(e)
-
+    if nz == 4:
+        upper = z // 2
+        inner = (z + upper) % 2
+        chips = [z, z + 1 - 2 * (z % 2), 2 - upper, 3 - 3 * upper]
+        goals = chips
+        places = [0, 1, 3 - inner, 3 - inner]
+        turn = [2, 3, 1, 0]
+    else:
+        chips = [(z + nz - g) % nz for g in range(nz)]
+        goals = [(z + g) % nz for g in range(nz)]
+        places = list(range(nz))
+        turn = [*range(1, nz), 0]
+    core = e % 2
+    partner = e + 1 - 2 * core
+
+    def at(pos):
+        return pl.ds(pl.multiple_of(pos * slot, slot), slot)
+
+    send(pick.at[block(partner)], xin.at[p, at(1)], z_sem.at[1], {"ep": partner})
+    for g in range(1, nz):
+        for c in range(2):
+            peer = 2 * goals[g] + c
+            mine = 2 * places[g] + core
+            send(pick.at[block(peer)], xin.at[p, at(mine)], z_sem.at[mine], {"ep": peer})
+    xin[p, at(0)] = pick[block(e), :]
+
+    def spread(pos):
+        ref = xin.at[p, at(pos)]
+        send(ref, ref, ag_sem.at[0, pos], to_x)
+        send(ref, ref, ag_sem.at[1, pos], to_y)
+
+    def forward(pos):
+        if pos % 2 == 0:
+            ref = xin.at[px, at(pos)]
+            arrive(ref, ag_sem.at[0, pos])
+            send(ref, ref, ag_sem.at[2, pos], to_y)
+        else:
+            ref = xin.at[py, at(pos)]
+            arrive(ref, ag_sem.at[1, pos])
+            send(ref, ref, ag_sem.at[2, pos], to_x)
+
+    spread(0)
     loads[1].wait()
     dhid[p] = silu(dot(tok[...], w_side[...])).astype(jnp.bfloat16)
+    arrive(xin.at[p, at(1)], z_sem.at[1])
+    spread(1)
     send(dhid.at[p], dhid.at[p], dh_sem.at[0], to_x)
     send(dhid.at[p], dhid.at[p], dh_sem.at[1], to_y)
 
@@ -217,18 +248,10 @@
     comb[0] = high
     comb[1] = (both - high.astype(jnp.float32)).astype(jnp.bfloat16)
 
-    near = [n_ep - k for k in far[::-1]]
-    near = sorted(range(1, n_ep), key=lambda k: min(k, n_ep - k))
-    for k in near:
-        owner = (e + n_ep - k) % n_ep
-        arrive(xin.at[p, block(owner)], z_sem.at[owner])
-        spread(owner)
-
     tile = 2 * LANES
     n_tiles = g_acc.shape[1] // tile
-
-    loads[2].wait()
-    loads[3].wait()
+    f32 = jnp.float32
+    half = tok_rows // 2
 
     def gate_up(q, first):
         rows = pl.ds(pl.multiple_of(q * width, width), width)
@@ -245,128 +268,123 @@
                 g_acc[:, cols] += g
                 u_acc[:, cols] += u
 
+    def gate_up_last(q):
+        rows = pl.ds(pl.multiple_of(q * width, width), width)
+
+        @pl.loop(0, n_tiles)
+        def _(n):
+            cols = pl.ds(pl.multiple_of(n * tile, tile), tile)
+            g = g_acc[:, cols] + dot(xin[q], w_gate[rows, cols])
+            u = u_acc[:, cols] + dot(xin[q], w_up[rows, cols])
+            hid[:, cols] = (silu(g) * u).astype(jnp.bfloat16)
+
+    def down(to, q):
+
+        @pl.loop(0, width // tile)
+        def _(n):
+            cols = pl.ds(pl.multiple_of(n * tile, tile), tile)
+            src = pl.ds(pl.multiple_of(q * width + n * tile, tile), tile)
+            part[to, :, cols] = dot(hid[...], w_down[:, src]).astype(jnp.bfloat16)
+
+    def wait_x():
+        for pos in range(n_ep):
+            if pos % 2:
+                arrive(xin.at[px, at(pos)], ag_sem.at[0, pos])
+
+    def wait_y():
+        for pos in range(n_ep):
+            if pos % 2 == 0:
+                arrive(xin.at[py, at(pos)], ag_sem.at[1, pos])
+
+    def wait_d():
+        for pos in range(n_ep):
+            arrive(xin.at[pd, at(pos)], ag_sem.at[2, pos])
+
+    def first_d(g):
+        even, odd = at(2 * g), at(2 * g + 1)
+        send(part.at[3, odd], d_in.at[odd], rsd_sem.at[2 * g + 1], to_x)
+        send(part.at[3, even], d_in.at[even], rsd_sem.at[2 * g], to_y)
+
+    def direct_x(g):
+        odd = at(2 * g + 1)
+        send(part.at[1, odd], rx.at[odd], rsx_sem.at[2 * g + 1], to_x)
+
+    def direct_y(g):
+        even = at(2 * g)
+        send(part.at[2, even], ry.at[even], rsy_sem.at[2 * g], to_y)
+
+    def joined(g):
+        for pos, src, dst, sem, there in (
+            (2 * g, 1, rx, rsx_sem, to_x),
+            (2 * g + 1, 2, ry, rsy_sem, to_y),
+        ):
+            b = at(pos)
+            arrive(d_in.at[b], rsd_sem.at[pos])
+            pair[b, :] = (part[src, b, :].astype(f32) + d_in[b, :].astype(f32)).astype(
+                jnp.bfloat16
+            )
+            send(pair.at[b], dst.at[b], sem.at[pos], there)
+
+    def finish(g):
+        for c in range(2):
+            pos = 2 * g + c
+            b = at(pos)
+            arrive(rx.at[b], rsx_sem.at[pos])
+            arrive(ry.at[b], rsy_sem.at[pos])
+            total = (
+                part[0, b, :].astype(f32) + rx[b, :].astype(f32) + ry[b, :].astype(f32)
+            ).astype(jnp.bfloat16)
+            if pos == 0:
+                back[block(e), :] = total
+            else:
+                fin[b, :] = total
+                owner = partner if g == 0 else 2 * chips[g] + c
+                send(fin.at[b], back.at[block(e)], ret_sem.at[e], {"ep": owner})
+
+    lag = n_ep
+    for pos in range(2, n_ep):
+        arrive(xin.at[p, at(pos)], z_sem.at[pos])
+        spread(pos)
+        if pos >= lag:
+            forward(pos - lag)
+    loads[2].wait()
+    loads[3].wait()
     gate_up(p, True)
-
-    order = [0] + near
-    zs = [j for j in range(nz)]
-    for j in zs:
-        zo = (z + j) % nz
-        even, odd = 2 * zo, 2 * zo + 1
-        ref = xin.at[px, block(even)]
-        arrive(ref, ag_sem.at[0, even])
-        send(ref, ref, ag_sem.at[2, even], to_y)
-        ref = xin.at[py, block(odd)]
-        arrive(ref, ag_sem.at[1, odd])
-        send(ref, ref, ag_sem.at[2, odd], to_x)
-    half = tok_rows // 2
+    for pos in range(n_ep - lag, n_ep):
+        forward(pos)
     arrive(dhid.at[px], dh_sem.at[0])
     ref = dhid.at[px, pl.ds(0, half)]
     send(ref, ref, dh_sem.at[2], to_y)
     arrive(dhid.at[py], dh_sem.at[1])
     ref = dhid.at[py, pl.ds(half, half)]
     send(ref, ref, dh_sem.at[3], to_x)
-
-    for j in zs:
-        odd = 2 * j + 1
-        arrive(xin.at[px, block(odd)], ag_sem.at[0, odd])
+    wait_x()
     gate_up(px, False)
-    for j in zs:
-        even = 2 * j
-        arrive(xin.at[py, block(even)], ag_sem.at[1, even])
+    wait_y()
     gate_up(py, False)
-    for owner in range(n_ep):
-        arrive(xin.at[pd, block(owner)], ag_sem.at[2, owner])
-
-    last = pl.ds(pl.multiple_of(pd * width, width), width)
-
-    @pl.loop(0, n_tiles)
-    def _(n):
-        cols = pl.ds(pl.multiple_of(n * tile, tile), tile)
-        g = g_acc[:, cols] + dot(xin[pd], w_gate[last, cols])
-        u = u_acc[:, cols] + dot(xin[pd], w_up[last, cols])
-        hid[:, cols] = (silu(g) * u).astype(jnp.bfloat16)
+    wait_d()
+    gate_up_last(pd)
 
     loads[4].wait()
-
-    def down(at, q):
-        @pl.loop(0, width // tile)
-        def _(n):
-            cols = pl.ds(pl.multiple_of(n * tile, tile), tile)
-            src = pl.ds(pl.multiple_of(q * width + n * tile, tile), tile)
-            part[at, :, cols] = dot(hid[...], w_down[:, src]).astype(jnp.bfloat16)
-
-    offs = sorted(range(nz), key=lambda j: (-min(j, nz - j), j))
-
-    def pieces(g):
-        zo = (z + offs[g]) % nz
-        return 2 * zo, 2 * zo + 1
-
-    def first_d(g):
-        even, odd = pieces(g)
-        send(part.at[3, block(odd)], d_in.at[block(odd)], rsd_sem.at[odd], to_x)
-        send(part.at[3, block(even)], d_in.at[block(even)], rsd_sem.at[even], to_y)
-
-    def direct_x(g):
-        odd = pieces(g)[1]
-        send(part.at[1, block(odd)], rx.at[block(odd)], rsx_sem.at[odd], to_x)
-
-    def direct_y(g):
-        even = pieces(g)[0]
-        send(part.at[2, block(even)], ry.at[block(even)], rsy_sem.at[even], to_y)
-
-    def direct(g):
-        first_d(g)
-        direct_x(g)
-        direct_y(g)
-
-    f32 = jnp.float32
-
-    def joined(g):
-        even, odd = pieces(g)
-        for owner, at, dst, sem, there in (
-            (even, 1, rx, rsx_sem, to_x),
-            (odd, 2, ry, rsy_sem, to_y),
-        ):
-            b = block(owner)
-            arrive(d_in.at[b], rsd_sem.at[owner])
-            pair[b, :] = (part[at, b, :].astype(f32) + d_in[b, :].astype(f32)).astype(
-                jnp.bfloat16
-            )
-            send(pair.at[b], dst.at[b], sem.at[owner], there)
-
-    def finish(g):
-        even, odd = pieces(g)
-        for owner in (even, odd):
-            b = block(owner)
-            arrive(rx.at[b], rsx_sem.at[owner])
-            arrive(ry.at[b], rsy_sem.at[owner])
-            fin[b, :] = (
-                part[0, b, :].astype(f32) + rx[b, :].astype(f32) + ry[b, :].astype(f32)
-            ).astype(jnp.bfloat16)
-            if offs[g]:
-                send(fin.at[b], back.at[block(e)], ret_sem.at[e], {"ep": owner})
-        if not offs[g]:
-            other = e + 1 - 2 * (e % 2)
-            send(fin.at[block(other)], back.at[block(e)], ret_sem.at[e], {"ep": other})
-            back[block(e), :] = fin[block(e), :]
-
     down(3, pd)
-    first_d(0)
+    first_d(turn[0])
+    first_d(turn[1])
     down(1, px)
-    direct_x(0)
+    direct_x(turn[0])
     down(2, py)
-    direct_y(0)
-    if nz > 1:
-        direct(1)
+    direct_y(turn[0])
+    direct_x(turn[1])
+    direct_y(turn[1])
     down(0, p)
-
-    for g in range(nz):
-        joined(g)
-        if g + 2 < nz:
-            direct(g + 2)
-        if g >= 1:
-            finish(g - 1)
-        if g == min(1, nz - 1):
+    for i in range(nz):
+        joined(turn[i])
+        if i + 2 < nz:
+            first_d(turn[i + 2])
+            direct_x(turn[i + 2])
+            direct_y(turn[i + 2])
+        if i >= 1:
+            finish(turn[i - 1])
+        if i == 1:
             arrive(dhid.at[pd, pl.ds(0, half)], dh_sem.at[2])
             arrive(dhid.at[pd, pl.ds(half, half)], dh_sem.at[3])
             loads[5].wait()
@@ -374,17 +392,19 @@
             for q in range(1, dhid.shape[0]):
                 total += dot(dhid[q], w_dout[pl.ds(q * side, side)])
             logit = jnp.sum(
-                tok[...].astype(f32) * dgate_ref[...].astype(f32), axis=1, keepdims=True
+                tok[...].astype(f32) * dgate_ref[...].reshape(1, tok.shape[1]).astype(f32),
+                axis=1,
+                keepdims=True,
             )
             g_acc[:, pl.ds(0, width)] = total / (1.0 + jnp.exp(-logit))
-    finish(nz - 1)
-
-    for k in near:
+    finish(turn[-1])
+
+    for k in range(1, n_ep):
         owner = (e + n_ep - k) % n_ep
         arrive(back.at[block(owner)], ret_sem.at[owner])
     out_ref[...] = (
         g_acc[:, pl.ds(0, width)] + dot(comb[0], back[...]) + dot(comb[1], back[...])
-    ).astype(jnp.bfloat16)
+    )
     for copy in sends:
         copy.wait_send()
 
@@ -413,7 +433,7 @@
     vmem = pl.BlockSpec(memory_space=pltpu.VMEM)
     return pl.pallas_call(
         functools.partial(layer_kernel, n_ep, slot),
-        out_shape=jax.ShapeDtypeStruct((tok_rows, width), bf16),
+        out_shape=pltpu.VMEM((tok_rows, width), f32),
         in_specs=[hbm] * 6 + [vmem] * 3,
         out_specs=vmem,
         scratch_shapes=[
@@ -455,10 +475,10 @@
         down_proj,
         side_input_weight,
         dense_out,
-        dense_gate.reshape(1, d),
+        dense_gate,
         chosen_rows,
         choice_weights,
-    )
+    ).astype(bf16)
 
 
 def per_device(*args):
@@ -468,7 +488,7 @@
     width, tile = tokens.shape[1] // n_tp, 2 * LANES
     fits = (
         n_tp == 4
-        and n_ep % 2 == 0
+        and n_ep % 4 == 0
         and tokens.shape[0] == n_ep * slot
         and slot % 16 == 0
         and width % tile == 0

time: 43.9 us -> 38.8 us (0.88)
  local copies, waits for them, and re-layouts: 2.96 us -> 0 us
  Pallas kernels: 40.6 us -> 37.9 us
  other arithmetic: 0 us -> 0.74 us
    pallas_call x1, Pallas kernels: 40.6 us -> 37.9 us  [fused_per_device(): pl.pallas_call(functools.partial(layer_kernel, n_ep, slot), out_shape=plt...]
    unnamed x1 -> x0, local copies, waits for them, and re-layouts: 1.67 us -> none
    reshape x1 -> x0, local copies, waits for them, and re-layouts: 1.29 us -> none  [fused_per_device(): dense_gate.reshape(1, d)]
    convert_element_type x0 -> x1, other arithmetic: none -> 0.74 us  [fused_per_device(): return pl.pallas_call(functools.partial(layer_kernel, n_ep, slot), out_sh...]
where the time goes in v2:
time: 38.8 us; the launch traced here: 38.6 us
  Pallas kernels  37.9 us (98%)
  other arithmetic  0.74 us (2%)
    pallas_call x1, Pallas kernels, fused_per_device(): pl.pallas_call(functools.partial(layer_kernel, n_ep, slot), out_shape=plt...  37.9 us

profile of v2, /device:TPU:0, one launch (start us, length us, event | category | flops | bytes accessed | tf_op | source)
XLA Modules:
  0.0 38.6 jit_solution(8225858460797818516)
XLA Ops:
  0.0 37.9 %shard_map.91 = f32[256,512]{1,0:T(8,128)S(1)} custom-call(bf16[256,2048]{1,0:T(8,128)(2,1)} %tok_hbm.1, bf16[1,2048,1024]{2,1,0:T(8,128)(2,1)} %gate_hbm.1, bf16[1,2048,1024]{2,1,0:T(8,128)(2,1)} %up_hbm.1, bf16[1,1024,2048]{2,1,0:T(8,128)(2,1)} %down_hbm.1, bf16[2048,256]{1,0:T(8,128)(2,1)} %side_hbm.1, bf16[1024,512]{1,0:T(8,128)(2,1)} %dout_hbm.1, ...), custom_call_target="tpu_custom_call" | custom-call | tf_op jit(solution)/shard_map/pallas_call | solution.py:434
  37.9 0.7 %convert_element_type.3 = bf16[256,512]{1,0:T(8,128)(2,1)} convert(f32[256,512]{1,0:T(8,128)S(1)} %shard_map.91) | non-fusion elementwise | flops 131072 | bytes 786432 | tf_op jit(solution)/shard_map/convert_element_type | solution.py:481

commit v3 on v2

--- a/solution.py
+++ b/solution.py
@@ -382,8 +382,8 @@
             first_d(turn[i + 2])
             direct_x(turn[i + 2])
             direct_y(turn[i + 2])
-        if i >= 1:
-            finish(turn[i - 1])
+        if i >= 2:
+            finish(turn[i - 2])
         if i == 1:
             arrive(dhid.at[pd, pl.ds(0, half)], dh_sem.at[2])
             arrive(dhid.at[pd, pl.ds(half, half)], dh_sem.at[3])
@@ -397,6 +397,7 @@
                 keepdims=True,
             )
             g_acc[:, pl.ds(0, width)] = total / (1.0 + jnp.exp(-logit))
+    finish(turn[-2])
     finish(turn[-1])
 
     for k in range(1, n_ep):

time: 38.8 us -> 39.6 us (1.021)
  Pallas kernels: 37.9 us -> 38.6 us
    pallas_call x1, Pallas kernels: 37.9 us -> 38.6 us  [fused_per_device(): pl.pallas_call(functools.partial(layer_kernel, n_ep, slot), out_shape=plt...]
where the time goes in v3:
time: 39.6 us; the launch traced here: 39.4 us
  Pallas kernels  38.6 us (97%)
  other arithmetic  0.74 us (2%)
    pallas_call x1, Pallas kernels, fused_per_device(): pl.pallas_call(functools.partial(layer_kernel, n_ep, slot), out_shape=plt...  38.6 us

profile of v3, /device:TPU:0, one launch (start us, length us, event | category | flops | bytes accessed | tf_op | source)
XLA Modules:
  0.0 39.4 jit_solution(11695947855667463275)
XLA Ops:
  0.0 38.6 %shard_map.91 = f32[256,512]{1,0:T(8,128)S(1)} custom-call(bf16[256,2048]{1,0:T(8,128)(2,1)} %tok_hbm.1, bf16[1,2048,1024]{2,1,0:T(8,128)(2,1)} %gate_hbm.1, bf16[1,2048,1024]{2,1,0:T(8,128)(2,1)} %up_hbm.1, bf16[1,1024,2048]{2,1,0:T(8,128)(2,1)} %down_hbm.1, bf16[2048,256]{1,0:T(8,128)(2,1)} %side_hbm.1, bf16[1024,512]{1,0:T(8,128)(2,1)} %dout_hbm.1, ...), custom_call_target="tpu_custom_call" | custom-call | tf_op jit(solution)/shard_map/pallas_call | solution.py:435
  38.6 0.7 %convert_element_type.3 = bf16[256,512]{1,0:T(8,128)(2,1)} convert(f32[256,512]{1,0:T(8,128)S(1)} %shard_map.91) | non-fusion elementwise | flops 131072 | bytes 786432 | tf_op jit(solution)/shard_map/convert_element_type | solution.py:482

commit v4 on v2

--- a/solution.py
+++ b/solution.py
@@ -382,8 +382,6 @@
             first_d(turn[i + 2])
             direct_x(turn[i + 2])
             direct_y(turn[i + 2])
-        if i >= 1:
-            finish(turn[i - 1])
         if i == 1:
             arrive(dhid.at[pd, pl.ds(0, half)], dh_sem.at[2])
             arrive(dhid.at[pd, pl.ds(half, half)], dh_sem.at[3])
@@ -397,6 +395,8 @@
                 keepdims=True,
             )
             g_acc[:, pl.ds(0, width)] = total / (1.0 + jnp.exp(-logit))
+        if i >= 1:
+            finish(turn[i - 1])
     finish(turn[-1])
 
     for k in range(1, n_ep):

time: 38.8 us -> 38.8 us (level)
  no operation moved by 1% of the time
where the time goes in v4:
time: 38.8 us; the launch traced here: 38.6 us
  Pallas kernels  37.9 us (98%)
  other arithmetic  0.74 us (2%)
    pallas_call x1, Pallas kernels, fused_per_device(): pl.pallas_call(functools.partial(layer_kernel, n_ep, slot), out_shape=plt...  37.9 us

profile of v4, /device:TPU:0, one launch (start us, length us, event | category | flops | bytes accessed | tf_op | source)
XLA Modules:
  0.0 38.6 jit_solution(5925798516811733777)
XLA Ops:
  0.0 37.9 %shard_map.91 = f32[256,512]{1,0:T(8,128)S(1)} custom-call(bf16[256,2048]{1,0:T(8,128)(2,1)} %tok_hbm.1, bf16[1,2048,1024]{2,1,0:T(8,128)(2,1)} %gate_hbm.1, bf16[1,2048,1024]{2,1,0:T(8,128)(2,1)} %up_hbm.1, bf16[1,1024,2048]{2,1,0:T(8,128)(2,1)} %down_hbm.1, bf16[2048,256]{1,0:T(8,128)(2,1)} %side_hbm.1, bf16[1024,512]{1,0:T(8,128)(2,1)} %dout_hbm.1, ...), custom_call_target="tpu_custom_call" | custom-call | tf_op jit(solution)/shard_map/pallas_call | solution.py:434
  37.9 0.7 %convert_element_type.3 = bf16[256,512]{1,0:T(8,128)(2,1)} convert(f32[256,512]{1,0:T(8,128)S(1)} %shard_map.91) | non-fusion elementwise | flops 131072 | bytes 786432 | tf_op jit(solution)/shard_map/convert_element_type | solution.py:481
